TPU v7x, 512 devices: a whole 4x8x8 slice. The times are simulated.
512 devices in a mesh: sp: 32 (over z, x), tp: 16 (over y, core).
Axes of the slice: x: 4, y: 8, z: 8, core: 2. Of those that a mesh axis runs over, the one named last changes fastest.
Arguments:
- tokens: bfloat16 [32, 3072, 2048], P('sp', 'tp'), may hold values from -100 to 100
- norm_gain: float32 [2048], replicated, may hold values from 0.1 to 1.9
- key_weight: bfloat16 [2048, 1024], P('sp', 'tp'), may hold values from -0.125 to 0.125
- value_weight: bfloat16 [2048, 1024], P('sp', 'tp'), may hold values from -0.125 to 0.125
- cum_gate: float32 [32, 32, 3072], P('sp', None, 'tp'), may hold values from -448 to 0, as said below
- new_gate: float32 [32, 32], P('sp', 'tp'), may hold values from -448 to 0
- new_query: bfloat16 [32, 2048], P('sp', 'tp'), may hold values from -128 to 128
- new_kv: bfloat16 [32, 16, 128], P('sp', 'tp'), may hold values from -4 to 4
Outputs:
- kv_cache: bfloat16 [32, 16, 3072, 128], P('sp', 'tp')
- gate_log_cache: float32 [32, 32, 3072], P('sp', 'tp')
- read_out: bfloat16 [32, 2048], P('sp', 'tp')
Inputs may be any that keep to these rules, and one draw needn't show every extreme that they name: Along positions cum_gate never rises; new_gate is at most the last position's value of its prompt and head.
All inputs are finite; a program needn't handle non-finite values.
Results may differ from a plain program's by a relative error of at most 0.0071.
Values may be sent and summed in bfloat16 or wider, within the bound.
No kernel may reach another device: no remote copies, remote signals or barrier semaphores. Data moves between devices by JAX's collectives and lax.ppermute only.
A program may use at most 64 MiB of HBM per device.

v0:
```python
import math
import jax
import jax.numpy as jnp
from jax import lax
from jax.sharding import PartitionSpec as P

HEAD = 64


def sent_together(arrays, axis, dim, along):
    widths = [a.shape[along] for a in arrays]
    both = jnp.concatenate(arrays, axis=along)
    filled = lax.all_gather(both, axis, axis=dim, tiled=True)
    return tuple(jnp.split(filled, [sum(widths[:k]) for k in range(1, len(widths))], axis=along))


def normalize(rows, norm_gain):
    widened = rows.astype(jnp.float32)
    inv_rms = lax.rsqrt(jnp.mean(widened * widened, axis=-1, keepdims=True) + 1e-06)
    scaled = (widened * norm_gain).astype(jnp.bfloat16)
    return (scaled, inv_rms)


def per_device(tokens, norm_gain, key_weight, value_weight, cum_gate, new_gate, new_query, new_kv):
    key_rows, value_rows = sent_together((key_weight, value_weight), "sp", 0, 1)
    prompts, positions, model_width = tokens.shape
    local_width = key_rows.shape[1]
    kv_here = local_width // HEAD
    gate_here = lax.all_to_all(cum_gate, "tp", split_axis=1, concat_axis=2, tiled=True)
    both_weights = jnp.concatenate([key_rows, value_rows], axis=1)
    piece = lax.all_gather(tokens, "tp", axis=1, tiled=True)
    scaled, inv_rms = normalize(piece, norm_gain)
    flat = scaled.reshape(-1, model_width)
    product = jnp.dot(flat, both_weights, preferred_element_type=jnp.float32)
    product = product.reshape(piece.shape[0], piece.shape[1], 2 * local_width) * inv_rms
    projected = product.astype(jnp.bfloat16)
    length = projected.shape[1]
    key_heads = projected[:, :, :local_width].reshape(prompts, length, kv_here, HEAD)
    value_heads = projected[:, :, local_width:].reshape(prompts, length, kv_here, HEAD)
    cache_local_copy = jnp.transpose(
        jnp.concatenate([key_heads, value_heads], axis=3), (0, 2, 1, 3)
    )
    length = cache_local_copy.shape[2]
    heads_here = gate_here.shape[1]
    group = heads_here // kv_here
    scale_factor = 1.0 / math.sqrt(HEAD)
    keys = cache_local_copy[..., :HEAD]
    values = cache_local_copy[..., HEAD:]
    query = new_query.reshape(prompts, kv_here, group, HEAD)
    own_key = new_kv[..., :HEAD].astype(jnp.float32)
    own_value = new_kv[..., HEAD:].astype(jnp.float32)
    score = (
        jnp.einsum("skgd,sktd->skgt", query, keys, preferred_element_type=jnp.float32)
        * scale_factor
    )
    score = (
        score
        + new_gate.reshape(prompts, kv_here, group)[..., None]
        - gate_here.reshape(prompts, kv_here, group, length)
    )
    own = jnp.sum(query.astype(jnp.float32) * own_key[:, :, None, :], axis=3) * scale_factor
    top = jnp.maximum(jnp.max(score, axis=3), own)
    expo = jnp.exp(score - top[..., None])
    own_factor = jnp.exp(own - top)
    total = jnp.sum(expo, axis=3) + own_factor
    weights = expo.astype(jnp.bfloat16)
    numer = jnp.einsum("skgt,sktd->skgd", weights, values, preferred_element_type=jnp.float32)
    numer = numer + own_factor[..., None] * own_value[:, :, None, :]
    read_out = (numer / total[..., None]).reshape(prompts, heads_here * HEAD).astype(jnp.bfloat16)
    return (cache_local_copy, gate_here, read_out)


def solution(mesh):
    in_specs = (
        P("sp", "tp", None),
        P(),
        P("sp", "tp"),
        P("sp", "tp"),
        P("sp", None, "tp"),
        P("sp", "tp"),
        P("sp", "tp"),
        P("sp", "tp", None),
    )
    out_specs = (P("sp", "tp", None, None), P("sp", "tp", None), P("sp", "tp"))
    return jax.shard_map(
        per_device, mesh=mesh, in_specs=in_specs, out_specs=out_specs, check_vma=False
    )
```

profile of v0, /device:TPU:1, one launch (start us, length us, event | category | flops | bytes accessed | tf_op | source)
XLA Modules:
  0.0 119.5 jit_solution(1385193337184464676)
XLA Ops:
  7.2 0.0 copy-start
  7.2 0.0 all-gather.2.cloned.1.call-start
  7.2 0.7 all-gather.2.cloned.1.call-update
  7.9 1.4 %copy.13 = f32[1,32,192]{2,0,1:T(1,128)} copy(f32[1,32,192]{2,1,0:T(8,128)} %param.12) | data formatting | bytes 49152 | tf_op args[4]
  9.3 10.1 %all-to-all-start = ((f32[1,32,192]{2,0,1:T(1,128)}), f32[1,32,192]{2,0,1:T(1,128)S(1)}, u32[]{:S(2)}, u32[]{:S(2)}) async-start(f32[1,32,192]{2,0,1:T(1,128)} %copy.13), calls=%async_computation | async-start | bytes 65536 | tf_op jit(solution)/shard_map/all_to_all | solution.py:29
  19.4 0.7 convert_reduce_fusion
  20.1 0.1 reshape.184
  20.2 0.8 pad_maximum_fusion
  21.0 47.1 %all_gather.7 = bf16[2048,128]{1,0:T(8,128)(2,1)S(1)} all-gather(bf16[64,128]{1,0:T(8,128)(2,1)S(1)} %pad_maximum_fusion), channel_id=1, replica_groups=mesh['sp'=32,'tp'=16] {'sp'}, dimensions={0}, use_global_device_ids=true | all-gather | bytes 540672 | tf_op jit(solution)/shard_map/all_gather | solution.py:13
  68.1 0.8 bitcast_convert_fusion
  68.9 0.1 multiply_reduce_fusion
  69.0 0.5 broadcast.78
  69.5 1.3 %reduce.13 = bf16[128]{0:T(256)(128)(2,1)S(1)} reduce(bf16[1,128]{1,0:T(2,128)(2,1)} %param.14, bf16[]{:T(256)} %broadcast.78), dimensions={0}, to_apply=%param.14.reduce_sub_computation.3 | reduce | bytes 514 | tf_op args[6]
  70.8 0.1 reshape.181
  70.9 0.0 all-to-all-done
  70.9 0.1 reshape.182
  71.0 0.7 all_to_all.16
  71.7 22.2 %all-gather.2.cloned.1.call-done = bf16[1,3072,2048]{2,1,0:T(8,128)(2,1)} async-done(((bf16[1,192,2048]{2,1,0:T(8,128)(2,1)}), bf16[1,3072,2048]{2,1,0:T(8,128)(2,1)}) %all-gather.2.cloned.1.call-update) | async-done | bytes 12582928 | tf_op jit(solution)/shard_map/all_gather | solution.py:31
  93.9 7.1 %fusion.1 = f32[3072]{0:T(1024)S(1)} fusion(bf16[1,3072,2048]{2,1,0:T(8,128)(2,1)} %all-gather.2.cloned.1.call-done), kind=kLoop, calls=%fused_computation.3 | loop fusion | flops 18871296 | bytes 12595200 | tf_op jit(solution)/shard_map/reduce_sum | solution.py:19
  101.0 0.0 copy-done
  101.0 0.0 copy-start.1
  101.1 8.9 %fusion.12 = bf16[1,3072,128]{1,2,0:T(8,128)(2,1)S(1)} fusion(bf16[2048,128]{1,0:T(8,128)(2,1)S(1)} %all_gather.7, bf16[1,3072,2048]{2,1,0:T(8,128)(2,1)} %all-gather.2.cloned.1.call-done, f32[2048]{0:T(1024)S(1)} %copy-done, f32[3072]{0:T(1024)S(1)} %add_rsqrt_fusion), kind=kOutput, calls=%fused_computation.9 | convolution fusion | flops 1630273536 | bytes 13914112 | tf_op jit(solution)/shard_map/dot_general | solution.py:34
  109.9 0.1 slice_bitcast_fusion.5
  110.0 0.1 maximum_bitcast_fusion
  110.1 1.2 copy.15
  111.2 0.0 copy-done.1
  111.2 0.3 fusion.24
  111.5 0.2 fusion.20
  111.7 0.3 fusion.19
  112.0 0.6 convert_element_type.57
  (4 shorter events, 0.0 us)
Async XLA Ops:
  7.2 93.9 %copy-start = (f32[2048]{0:T(1024)S(1)}, f32[2048]{0:T(1024)}, u32[]{:S(2)}) copy-start(f32[2048]{0:T(1024)} %param.9) | copy-start | bytes 24580
  7.2 86.8 %all-gather.2.cloned.1.call-start = ((), (), s32[]{:S(2)}) async-start(), calls=%async_computation.1 | async-start | bytes 13369344 | tf_op jit(solution)/shard_map/all_gather | solution.py:31
  9.3 61.6 %all-to-all-start = ((f32[1,32,192]{2,0,1:T(1,128)}), f32[1,32,192]{2,0,1:T(1,128)S(1)}, u32[]{:S(2)}, u32[]{:S(2)}) async-start(f32[1,32,192]{2,0,1:T(1,128)} %copy.13), calls=%async_computation | async-start | bytes 65536 | tf_op jit(solution)/shard_map/all_to_all | solution.py:29
  101.0 10.2 %copy-start.1 = (f32[1,2]{1,0:T(1,128)S(1)}, f32[1,2]{1,0:T(1,128)}, u32[]{:S(2)}) copy-start(f32[1,2]{1,0:T(1,128)} %param.13) | copy-start | bytes 28
Sparse Core Ops, SparseCore 0:
  10.1 83.7 all-gather.1
where the time goes:
time: 120 us; the launch traced here: 119 us
  blocking collectives  47.1 us (39%)
  waiting for transfers between devices  22.9 us (19%)
  between operations  14.1 us (12%)
  other arithmetic  11.1 us (9%)
  starting transfers between devices  10.2 us (8%)
  matrix products  9.43 us (8%)
  local copies, waits for them, and re-layouts  4.71 us (4%)
    all_gather x1, blocking collectives, sent_together(): filled = lax.all_gather(both, axis, axis=dim, tiled=True)  47.1 us
    all_gather x1, waiting for transfers between devices, per_device(): piece = lax.all_gather(tokens, 'tp', axis=1, tiled=True)  22.2 us
    all_to_all x1, starting transfers between devices, per_device(): lax.all_to_all(cum_gate, 'tp', split_axis=1, concat_axis=2, tiled=True)  10.1 us
    dot_general x1, matrix products, per_device(): product = jnp.dot(flat, both_weights, preferred_element_type=jnp.float32)  8.88 us
    reduce_sum x1, other arithmetic, normalize(): jnp.mean(widened * widened, axis=-1, keepdims=True) + 1e-06  7.09 us
    unnamed x7, local copies, waits for them, and re-layouts  3.09 us
  transfers between devices with their start and end apart: 2, of which 1 were waited for; matrix products, arithmetic and copies ran while one was open for 5% of the time, Pallas kernels for 0%

commit v1 on v0

--- a/solution.py
+++ b/solution.py
@@ -28,7 +28,8 @@
     kv_here = local_width // HEAD
     gate_here = lax.all_to_all(cum_gate, "tp", split_axis=1, concat_axis=2, tiled=True)
     both_weights = jnp.concatenate([key_rows, value_rows], axis=1)
-    piece = lax.all_gather(tokens, "tp", axis=1, tiled=True)
+    sent = jnp.stack([tokens] * lax.axis_size("tp"))
+    piece = jnp.concatenate(lax.all_to_all(sent, "tp", 0, 0), axis=1)
     scaled, inv_rms = normalize(piece, norm_gain)
     flat = scaled.reshape(-1, model_width)
     product = jnp.dot(flat, both_weights, preferred_element_type=jnp.float32)

time: 120 us -> 325 us (2.71)
  waiting for transfers between devices: 22.9 us -> 223 us
  blocking collectives: 47.1 us -> 64.4 us
  between operations: 14.1 us -> 0.71 us
  local copies, waits for them, and re-layouts: 4.71 us -> 11.4 us
  starting transfers between devices: 10.2 us -> 5.2 us
  matrix products: 9.43 us -> 4.84 us
  other arithmetic: 11.1 us -> 14.6 us
    all_to_all x1, waiting for transfers between devices: 0.01 us -> 223 us  [per_device(): piece = jnp.concatenate(lax.all_to_all(sent, 'tp', 0, 0), axis=1)]
    all_gather x1 -> x0, waiting for transfers between devices: 22.2 us -> none  [per_device(): piece = lax.all_gather(tokens, 'tp', axis=1, tiled=True)]
    all_to_all x0 -> x1, blocking collectives: none -> 16.7 us  [per_device(): lax.all_to_all(cum_gate, 'tp', split_axis=1, concat_axis=2, tiled=True)]
    another operation x1 -> x2, local copies, waits for them, and re-layouts: 0.09 us -> 7.3 us  [the longest x1 7.21 us: per_device(): sent = jnp.stack([tokens] * lax.axis_size('tp'))]
    convert_element_type x0 -> x1, other arithmetic: none -> 6.23 us  [normalize(): scaled = (widened * norm_gain).astype(jnp.bfloat16)]
    all_to_all x1, starting transfers between devices: 10.1 us -> 5.2 us  [per_device(): piece = jnp.concatenate(lax.all_to_all(sent, 'tp', 0, 0), axis=1)]
    dot_general x1, matrix products: 8.88 us -> 4.28 us  [per_device(): product = jnp.dot(flat, both_weights, preferred_element_type=jnp.float32)]
  transfers between devices with their start and end apart: 2 -> 1, of which waited for: 1 -> 1; matrix products, arithmetic and copies ran while one was open for 5% -> 1% of each run, Pallas kernels for 0% -> 0%
where the time goes in v1:
time: 325 us; the launch traced here: 324 us
  waiting for transfers between devices  223 us (69%)
  blocking collectives  64.4 us (20%)
  other arithmetic  14.6 us (4%)
  local copies, waits for them, and re-layouts  11.4 us (4%)
  starting transfers between devices  5.2 us (2%)
  matrix products  4.84 us (1%)
    all_to_all x1, waiting for transfers between devices, per_device(): piece = jnp.concatenate(lax.all_to_all(sent, 'tp', 0, 0), axis=1)  223 us
    all_gather x1, blocking collectives, sent_together(): filled = lax.all_gather(both, axis, axis=dim, tiled=True)  47.7 us
    all_to_all x1, blocking collectives, per_device(): lax.all_to_all(cum_gate, 'tp', split_axis=1, concat_axis=2, tiled=True)  16.7 us
    another operation x1, local copies, waits for them, and re-layouts, per_device(): sent = jnp.stack([tokens] * lax.axis_size('tp'))  7.21 us
    reduce_sum x1, other arithmetic, normalize(): jnp.mean(widened * widened, axis=-1, keepdims=True) + 1e-06  7.11 us
  transfers between devices with their start and end apart: 1, of which 1 were waited for; matrix products, arithmetic and copies ran while one was open for 1% of the time, Pallas kernels for 0%

profile of v1, /device:TPU:1, one launch (start us, length us, event | category | flops | bytes accessed | tf_op | source)
XLA Modules:
  0.0 324.3 jit_solution(6760502813533942389)
XLA Ops:
  0.6 0.8 copy.16
  1.4 16.7 %all_to_all.23 = f32[1,32,192]{2,0,1:T(1,128)S(1)} all-to-all(f32[1,32,192]{2,0,1:T(1,128)S(1)} %copy.16), channel_id=1, replica_groups=mesh['sp'=32,'tp'=16] {'tp'}, dimensions={1} | all-to-all | bytes 49152 | tf_op jit(solution)/shard_map/all_to_all | solution.py:29
  18.1 7.2 %stack.2 = bf16[16,1,192,2048]{3,2,1,0:T(8,128)(2,1)} broadcast(bf16[192,2048]{1,0:T(8,128)(2,1)} %bitcast.43), dimensions={2,3} | broadcast | bytes 13369344 | tf_op jit(solution)/shard_map/stack | solution.py:31
  25.3 0.0 copy-start.4
  25.4 0.0 copy-start.3
  25.4 0.0 copy-start
  25.4 0.0 copy-start.1
  25.4 5.2 %all-to-all-start = ((bf16[16,1,192,2048]{3,2,1,0:T(8,128)(2,1)}), bf16[16,1,192,2048]{3,2,1,0:T(8,128)(2,1)}, u32[]{:S(2)}, u32[]{:S(2)}) async-start(bf16[16,1,192,2048]{3,2,1,0:T(8,128)(2,1)} %stack.2), calls=%async_computation | async-start | bytes 25165824 | tf_op jit(solution)/shard_map/all_to_all | solution.py:32
  30.6 0.0 copy-start.2
  30.6 0.5 broadcast.91
  31.1 0.0 copy-done.4
  31.1 0.7 reduce.14
  31.7 0.1 reshape.210
  31.9 0.1 reshape.214
  31.9 0.0 copy-done.3
  31.9 0.1 bitcast_convert_fusion
  32.0 0.1 multiply_reduce_fusion.1
  32.1 0.0 copy-done
  32.1 0.0 copy-done.1
  32.1 0.1 pad_maximum_fusion
  32.2 47.7 %all_gather.3 = bf16[2048,128]{1,0:T(8,128)(2,1)S(1)} all-gather(bf16[64,128]{1,0:T(8,128)(2,1)S(1)} %pad_maximum_fusion), channel_id=1, replica_groups=mesh['sp'=32,'tp'=16] {'sp'}, dimensions={0}, use_global_device_ids=true | all-gather | bytes 540672 | tf_op jit(solution)/shard_map/all_gather | solution.py:13
  79.9 0.1 reshape.211
  80.0 0.7 all_to_all.20
  80.7 223.2 %all-to-all-done = bf16[16,1,192,2048]{3,2,1,0:T(8,128)(2,1)} async-done(((bf16[16,1,192,2048]{3,2,1,0:T(8,128)(2,1)}), bf16[16,1,192,2048]{3,2,1,0:T(8,128)(2,1)}, u32[]{:S(2)}, u32[]{:S(2)}) %all-to-all-start) | async-done | bytes 12582944 | tf_op jit(solution)/shard_map/all_to_all | solution.py:32
  303.9 7.1 %multiply_reduce_fusion = f32[16,192]{1,0:T(8,128)S(1)} fusion(bf16[16,1,192,2048]{3,2,1,0:T(8,128)(2,1)} %all-to-all-done), kind=kLoop, calls=%fused_computation.2 | loop fusion | flops 18871296 | bytes 12595200 | tf_op jit(solution)/shard_map/reduce_sum | solution.py:19
  311.0 0.1 rsqrt.12
  311.1 0.0 copy-done.2
  311.1 6.2 %fusion = bf16[3072,2048]{1,0:T(8,128)(2,1)S(1)} fusion(f32[2048]{0:T(1024)S(1)} %copy-done.2, bf16[16,1,192,2048]{3,2,1,0:T(8,128)(2,1)} %all-to-all-done), kind=kLoop, calls=%fused_computation.1 | loop fusion | flops 18874368 | bytes 25174016 | tf_op jit(solution)/shard_map/convert_element_type | solution.py:20
  317.3 0.0 copy-start.5
  317.3 4.3 %fusion.2 = bf16[1,3072,128]{1,2,0:T(8,128)(2,1)S(1)} fusion(bf16[3072,2048]{1,0:T(8,128)(2,1)S(1)} %fusion, bf16[2048,128]{1,0:T(8,128)(2,1)S(1)} %all_gather.3, f32[3072]{0:T(1024)S(1)} %rsqrt.12), kind=kOutput, calls=%fused_computation.5 | convolution fusion | flops 1611399168 | bytes 13905920 | tf_op jit(solution)/shard_map/dot_general | solution.py:35
  321.6 0.1 slice_bitcast_fusion.5
  321.7 0.1 maximum_bitcast_fusion
  321.8 1.2 copy.18
  322.9 0.0 copy-done.5
  322.9 0.3 fusion.12
  323.2 0.2 fusion.8
  323.4 0.3 fusion.7
  323.7 0.6 convert_element_type.72
  (5 shorter events, 0.1 us)
Async XLA Ops:
  25.3 5.7 %copy-start.4 = (bf16[1,128]{1,0:T(2,128)(2,1)S(1)}, bf16[1,128]{1,0:T(2,128)(2,1)}, u32[]{:S(2)}) copy-start(bf16[1,128]{1,0:T(2,128)(2,1)} %param.14) | copy-start | bytes 772
  25.4 6.6 %copy-start.3 = (bf16[1,1,128]{2,1,0:T(2,128)(2,1)S(1)}, bf16[1,1,128]{2,1,0:T(2,128)(2,1)}, u32[]{:S(2)}) copy-start(bf16[1,1,128]{2,1,0:T(2,128)(2,1)} %param.15) | copy-start | bytes 772
  25.4 6.8 %copy-start = (bf16[64,64]{1,0:T(8,128)(2,1)S(1)}, bf16[64,64]{1,0:T(8,128)(2,1)}, u32[]{:S(2)}) copy-start(bf16[64,64]{1,0:T(8,128)(2,1)} %param.11) | copy-start | bytes 24580
  25.4 6.8 %copy-start.1 = (bf16[64,64]{1,0:T(8,128)(2,1)S(1)}, bf16[64,64]{1,0:T(8,128)(2,1)}, u32[]{:S(2)}) copy-start(bf16[64,64]{1,0:T(8,128)(2,1)} %param.10) | copy-start | bytes 24580
  25.4 278.5 %all-to-all-start = ((bf16[16,1,192,2048]{3,2,1,0:T(8,128)(2,1)}), bf16[16,1,192,2048]{3,2,1,0:T(8,128)(2,1)}, u32[]{:S(2)}, u32[]{:S(2)}) async-start(bf16[16,1,192,2048]{3,2,1,0:T(8,128)(2,1)} %stack.2), calls=%async_computation | async-start | bytes 25165824 | tf_op jit(solution)/shard_map/all_to_all | solution.py:32
  30.6 280.5 %copy-start.2 = (f32[2048]{0:T(1024)S(1)}, f32[2048]{0:T(1024)}, u32[]{:S(2)}) copy-start(f32[2048]{0:T(1024)} %param.9) | copy-start | bytes 24580
  317.3 5.6 %copy-start.5 = (f32[1,2]{1,0:T(1,128)S(1)}, f32[1,2]{1,0:T(1,128)}, u32[]{:S(2)}) copy-start(f32[1,2]{1,0:T(1,128)} %param.13) | copy-start | bytes 28
